TPU v7x, 32 devices: a whole 2x2x4 slice. The times are simulated.
32 devices in a mesh: ep: 8 (over z, core), tp: 4 (over y, x).
Axes of the slice: x: 2, y: 2, z: 4, core: 2. Of those that a mesh axis runs over, the one named last changes fastest.
Arguments:
- compressed_query: bfloat16 [1024, 1536], P('ep'), may hold values from -6 to 6
- compressed_key_value: bfloat16 [1024, 512], P('ep'), may hold values from -6 to 6
- rotary_key: bfloat16 [1024, 32], P('ep'), may hold values from -600 to 600
- query_norm_scale: float32 [1536], replicated, may hold values from 0.1 to 1.9
- context_norm_scale: float32 [512], replicated, may hold values from 0.1 to 1.9
- query_plain_weight: bfloat16 [1536, 1024], P(None, 'tp'), may hold values from -0.375 to 0.375
- query_rotary_weight: bfloat16 [1536, 512], P(None, 'tp'), may hold values from -0.375 to 0.375
- key_up_weight: bfloat16 [512, 1024], P(None, 'tp'), may hold values from -0.25 to 0.25
- value_up_weight: bfloat16 [512, 1024], P(None, 'tp'), may hold values from -0.25 to 0.25
- output_weight: bfloat16 [1024, 2048], P(None, 'tp'), may hold values from -0.75 to 0.75
- mixture_input: bfloat16 [1024, 2048], P('ep'), may hold values from -6 to 6
- mixture_gain: float32 [2048], replicated, may hold values from 0.1 to 1.9
- routes: int32 [1024, 2], P('ep'), may hold values from 0 to 7, all different within a row; in each aligned block of 128 rows (0 to 127, 128 to 255, ...) at most 48 rows name the same one
- route_weight: float32 [1024, 2], P('ep'), may hold values from 0.2 to 2
- expert_gate: bfloat16 [8, 2048, 4096], P('ep', None, 'tp'), may hold values from -0.125 to 0.125
- expert_up: bfloat16 [8, 2048, 4096], P('ep', None, 'tp'), may hold values from -0.125 to 0.125
- expert_down: bfloat16 [8, 4096, 2048], P('ep', None, 'tp'), may hold values from -0.09375 to 0.09375
- shared_gate: bfloat16 [2048, 512], P(None, 'tp'), may hold values from -0.125 to 0.125
- shared_up: bfloat16 [2048, 512], P(None, 'tp'), may hold values from -0.125 to 0.125
- shared_down: bfloat16 [512, 2048], P(None, 'tp'), may hold values from -0.25 to 0.25
Outputs:
- attended: bfloat16 [1024, 2048], P('ep', 'tp')
- combined: bfloat16 [1024, 2048], P('ep', 'tp')
Inputs may be any that keep to these rules, and one draw needn't show every extreme that they name: `routes`: in the rows of each index of ep, no expert is named more than 48 times, a bound that some block reaches there.
All inputs are finite; a program needn't handle non-finite values.
Results may differ from a plain program's by a relative error of at most 0.012.
The roundings to bfloat16 on the way count: a program that leaves them out, or rounds other values in their place, can miss the bound.
Values may be sent and summed in bfloat16 or wider, within the bound.
No kernel may reach another device: no remote copies, remote signals or barrier semaphores. Data moves between devices by JAX's collectives and lax.ppermute only.
A program may use at most 64 MiB of HBM per device.

v0:
```python
import math
import jax
import jax.numpy as jnp
from jax import lax
from jax.sharding import PartitionSpec as P

PLAIN_HEAD_SIZE = 64
ROTARY_SIZE = 32
VALUE_HEAD_SIZE = 64
TOPK = 2


def normed_rows(values, scaling):
    floats = values.astype(jnp.float32)
    return floats * lax.rsqrt(jnp.mean(floats * floats, axis=-1, keepdims=True) + 1e-06) * scaling


def rotary_tables(positions):
    inverse = 1.0 / 10000.0 ** (jnp.arange(0, ROTARY_SIZE, 2, dtype=jnp.float32) / ROTARY_SIZE)
    angles = positions.astype(jnp.float32)[:, None] * inverse[None, :]
    return (jnp.cos(angles), jnp.sin(angles))


def rotate(vectors, cosine, sine_part):
    half_width = vectors.shape[-1] // 2
    front_half = vectors[..., :half_width]
    back_half = vectors[..., half_width:]
    return jnp.concatenate(
        [front_half * cosine - back_half * sine_part, front_half * sine_part + back_half * cosine],
        axis=-1,
    )


def fold_blocks(carry_state, members, handle):
    length = members[0].shape[0]
    block_rows = math.gcd(length, 2048)

    def advance(block_index, carried):
        sliced = tuple(
            (
                lax.dynamic_slice_in_dim(member, block_index * block_rows, block_rows, 0)
                for member in members
            )
        )
        return handle(carried, sliced, block_index * block_rows)

    return lax.fori_loop(0, length // block_rows, advance, carry_state)


def per_device(
    compressed_query,
    compressed_key_value,
    rotary_key,
    query_norm_scale,
    context_norm_scale,
    query_plain_weight,
    query_rotary_weight,
    key_up_weight,
    value_up_weight,
    output_weight,
    mixture_input,
    mixture_gain,
    routes,
    route_weight,
    expert_gate,
    expert_up,
    expert_down,
    shared_gate,
    shared_up,
    shared_down,
):
    tokens = compressed_query.shape[0]
    heads_here = query_plain_weight.shape[1] // PLAIN_HEAD_SIZE
    offset = lax.axis_index("ep") * tokens
    cosine, sine_part = rotary_tables(offset + jnp.arange(tokens, dtype=jnp.int32))
    compressed = normed_rows(compressed_query, query_norm_scale).astype(jnp.bfloat16)
    query_nope = jnp.dot(compressed, query_plain_weight, preferred_element_type=jnp.float32)
    query_nope = query_nope.astype(jnp.bfloat16).reshape(tokens, heads_here, PLAIN_HEAD_SIZE)
    query_turn = jnp.dot(compressed, query_rotary_weight, preferred_element_type=jnp.float32)
    query_turn = query_turn.reshape(tokens, heads_here, ROTARY_SIZE)
    query_rot = rotate(query_turn, cosine[:, None, :], sine_part[:, None, :])
    context = normed_rows(compressed_key_value, context_norm_scale).astype(jnp.bfloat16)
    scale = (PLAIN_HEAD_SIZE + ROTARY_SIZE) ** (-0.5)
    start_state = (
        jnp.full((heads_here, tokens), -1e30, jnp.float32),
        jnp.zeros((heads_here, tokens), jnp.float32),
        jnp.zeros((heads_here, tokens, VALUE_HEAD_SIZE), jnp.float32),
    )

    def attend(carry_state, sliced, first_row):
        key_rows, value_rows, raw_turn = sliced
        count = raw_turn.shape[0]
        key_cos, key_sin = rotary_tables(first_row + jnp.arange(count, dtype=jnp.int32))
        turned = rotate(raw_turn.astype(jnp.float32), key_cos, key_sin)
        running_max, running_total, running_sum = carry_state
        key_heads = key_rows.reshape(count, heads_here, PLAIN_HEAD_SIZE)
        value_heads = value_rows.reshape(count, heads_here, VALUE_HEAD_SIZE)
        scores = (
            jnp.einsum("qhe,khe->hqk", query_nope, key_heads, preferred_element_type=jnp.float32)
            + jnp.einsum("qhr,kr->hqk", query_rot, turned, precision=lax.Precision.HIGHEST)
        ) * scale
        new_max = jnp.maximum(running_max, jnp.max(scores, axis=-1))
        factor = jnp.exp(running_max - new_max)
        weights = jnp.exp(scores - new_max[..., None])
        running_total = running_total * factor + jnp.sum(weights, axis=-1)
        running_sum = running_sum * factor[..., None] + jnp.einsum(
            "hqk,khe->hqe",
            weights.astype(jnp.bfloat16),
            value_heads,
            preferred_element_type=jnp.float32,
        )
        return (new_max, running_total, running_sum)

    def expand(carry_state, sliced, first_row):
        latent_rows, raw_turn = sliced
        key_rows = jnp.dot(latent_rows, key_up_weight, preferred_element_type=jnp.float32).astype(
            jnp.bfloat16
        )
        value_rows = jnp.dot(
            latent_rows, value_up_weight, preferred_element_type=jnp.float32
        ).astype(jnp.bfloat16)
        return attend(carry_state, (key_rows, value_rows, raw_turn), first_row)

    final_state = fold_blocks(
        start_state,
        (
            lax.all_gather(context, "ep", axis=0, tiled=True),
            lax.all_gather(rotary_key, "ep", axis=0, tiled=True),
        ),
        expand,
    )
    heads_out = final_state[2] / final_state[1][..., None]
    heads_out = (
        heads_out.transpose(1, 0, 2)
        .reshape(tokens, heads_here * VALUE_HEAD_SIZE)
        .astype(jnp.bfloat16)
    )
    all_heads = lax.all_gather(heads_out, "tp", axis=1, tiled=True)
    attended = jnp.dot(all_heads, output_weight, preferred_element_type=jnp.float32).astype(
        jnp.bfloat16
    )
    floats = mixture_input.astype(jnp.float32)
    centred = floats - jnp.mean(floats, axis=-1, keepdims=True)
    normed = (
        centred
        * lax.rsqrt(jnp.mean(centred * centred, axis=-1, keepdims=True) + 1e-05)
        * mixture_gain
    ).astype(jnp.bfloat16)
    experts = lax.axis_size("ep")
    rows_here = mixture_input.shape[0]
    model_width = normed.shape[1]
    capacity = rows_here * TOPK * 3 // (2 * experts)
    flat_routes = routes.reshape(-1)
    one_hot = (flat_routes[:, None] == jnp.arange(experts, dtype=jnp.int32)[None, :]).astype(
        jnp.int32
    )
    ranks = jnp.sum(one_hot * (jnp.cumsum(one_hot, axis=0) - 1), axis=1)
    slots = flat_routes * capacity + ranks
    owners = jnp.full((experts * capacity,), rows_here, jnp.int32)
    owners = owners.at[slots].set(jnp.arange(rows_here * TOPK, dtype=jnp.int32) // TOPK)
    padded = jnp.concatenate([normed, jnp.zeros((1, model_width), jnp.bfloat16)], axis=0)
    outgoing = padded[owners].reshape(experts, capacity, model_width)
    arrived = lax.all_to_all(outgoing, "ep", split_axis=0, concat_axis=0, tiled=True).reshape(
        experts * capacity, model_width
    )
    hidden = (
        jax.nn.silu(jnp.dot(arrived, expert_gate[0], preferred_element_type=jnp.float32))
        * jnp.dot(arrived, expert_up[0], preferred_element_type=jnp.float32)
    ).astype(jnp.bfloat16)
    shared_hidden = (
        jax.nn.silu(jnp.dot(normed, shared_gate, preferred_element_type=jnp.float32))
        * jnp.dot(normed, shared_up, preferred_element_type=jnp.float32)
    ).astype(jnp.bfloat16)
    all_hidden, all_shared = (
        lax.all_gather(hidden, "tp", axis=1, tiled=True),
        lax.all_gather(shared_hidden, "tp", axis=1, tiled=True),
    )
    expert_rows = jnp.dot(all_hidden, expert_down[0], preferred_element_type=jnp.float32).astype(
        jnp.bfloat16
    )
    features = expert_rows.shape[1]
    returned = lax.all_to_all(
        expert_rows.reshape(experts, capacity, features),
        "ep",
        split_axis=0,
        concat_axis=0,
        tiled=True,
    )
    picked = returned.reshape(experts * capacity, features)[slots]
    picked = picked.astype(jnp.float32).reshape(rows_here, TOPK, features)
    routed = jnp.sum(picked * route_weight[:, :, None], axis=1)
    combined = (
        jnp.dot(all_shared, shared_down, preferred_element_type=jnp.float32) + routed
    ).astype(jnp.bfloat16)
    return (attended, combined)


def solution(mesh):
    in_specs = (
        P("ep", None),
        P("ep", None),
        P("ep", None),
        P(),
        P(),
        P(None, "tp"),
        P(None, "tp"),
        P(None, "tp"),
        P(None, "tp"),
        P(None, "tp"),
        P("ep", None),
        P(),
        P("ep", None),
        P("ep", None),
        P("ep", None, "tp"),
        P("ep", None, "tp"),
        P("ep", None, "tp"),
        P(None, "tp"),
        P(None, "tp"),
        P(None, "tp"),
    )
    out_specs = (P("ep", "tp"), P("ep", "tp"))
    return jax.shard_map(
        per_device, mesh=mesh, in_specs=in_specs, out_specs=out_specs, check_vma=False
    )
```

profile of v0, /device:TPU:0, one launch (start us, length us, event | category | flops | bytes accessed | tf_op | source)
XLA Modules:
  0.0 154.8 jit_solution(1504360362727506415)
XLA Ops:
  7.2 0.0 copy-start
  7.2 0.9 copy.28
  8.1 0.1 eq.29
  8.2 0.1 eq.25
  8.3 0.7 broadcast_multiply_fusion
  9.0 0.6 reduce-window.6
  9.6 0.2 slice_reduce_fusion
  9.9 0.1 copy.27
  10.0 0.1 mul.279
  10.1 0.1 fusion.46
  10.2 1.4 scatter_custom_fusion
  11.7 1.2 convert_reduce_fusion
  12.9 1.3 fusion.21
  14.2 1.4 fusion.23
  15.6 0.1 concatenate.12
  15.7 3.1 %gather_fusion = bf16[384,2048]{1,0:T(8,128)(2,1)} fusion(bf16[129,2048]{1,0:T(8,128)(2,1)S(1)} %concatenate.12, s32[1024]{0:T(1024)S(1)} %pad_clamp_fusion.1), kind=kCustom, calls=%fused_computation | custom fusion | bytes 3147264 | tf_op jit(solution)/shard_map/gather | solution.py:162
  18.8 6.5 %all-to-all-start = ((bf16[8,48,2048]{2,1,0:T(8,128)(2,1)}), bf16[8,48,2048]{2,1,0:T(8,128)(2,1)S(1)}, u32[]{:S(2)}, u32[]{:S(2)}) async-start(bf16[8,48,2048]{2,1,0:T(8,128)(2,1)} %bitcast.14), calls=%async_computation | async-start | bytes 3145728 | tf_op jit(solution)/shard_map/all_to_all | solution.py:163
  25.3 0.0 all-gather.3.cloned.1.call-start
  25.4 0.1 fusion.29
  25.5 0.0 copy-done.11
  25.5 0.8 fusion.31
  26.2 0.0 all-gather.3.cloned.1.call-update
  26.3 0.0 all-gather.5.cloned.1.call-start
  26.3 45.2 %all-to-all-done = bf16[8,48,2048]{2,1,0:T(8,128)(2,1)S(1)} async-done(((bf16[8,48,2048]{2,1,0:T(8,128)(2,1)}), bf16[8,48,2048]{2,1,0:T(8,128)(2,1)S(1)}, u32[]{:S(2)}, u32[]{:S(2)}) %all-to-all-start) | async-done | bytes 1572896 | tf_op jit(solution)/shard_map/all_to_all | solution.py:163
  71.5 4.1 %fusion.4 = f32[384,1024]{1,0:T(8,128)S(1)} fusion(bf16[384,2048]{1,0:T(8,128)(2,1)S(1)} %bitcast.76, bf16[1,2048,1024]{2,1,0:T(8,128)(2,1)} %param.34), kind=kOutput, calls=%fused_computation.7 | convolution fusion | flops 1610612736 | bytes 7340032 | tf_op jit(solution)/shard_map/dot_general | solution.py:167
  75.7 0.0 copy-start.6
  75.7 0.0 copy-start.16
  75.7 2.9 %multiply_convert_fusion = bf16[384,1024]{1,0:T(8,128)(2,1)} fusion(f32[384,1024]{1,0:T(8,128)S(1)} %fusion.4, bf16[384,2048]{1,0:T(8,128)(2,1)S(1)} %bitcast.77, bf16[1,2048,1024]{2,1,0:T(8,128)(2,1)S(1)} %copy-done.13), kind=kOutput, calls=%fused_computation.14 | convolution fusion | flops 1612972032 | bytes 8126464 | tf_op jit(solution)/shard_map/dot_general | solution.py:168
  78.6 0.0 all-gather.5.cloned.1.call-update
  78.6 0.0 copy-done.6
  78.6 0.2 fusion.26
  78.8 1.6 %convolution_convert_fusion.3 = bf16[128,256]{1,0:T(8,128)(2,1)S(1)} fusion(bf16[1536,256]{1,0:T(8,128)(2,1)} %param.25, bf16[128,1536]{1,0:T(8,128)(2,1)S(1)} %copy-done.6, f32[1536]{0:T(1024)S(1)} %copy-done.16, f32[128]{0:T(128)S(1)} %add_rsqrt_fusion.2), kind=kOutput, calls=%fused_computation.28 | convolution fusion | flops 101482496 | bytes 1251840 | tf_op jit(solution)/shard_map/dot_general | solution.py:77
  80.4 0.1 copy.25
  80.5 0.0 copy-done.10
  80.5 0.0 copy-start.7
  80.5 12.8 %all_gather.16 = bf16[1024,32]{0,1:T(8,128)(2,1)S(1)} all-gather(bf16[128,32]{0,1:T(8,128)(2,1)S(1)} %copy-done.10), channel_id=1, replica_groups=mesh['ep'=8,'tp'=4] {'ep'}, dimensions={0}, use_global_device_ids=true | all-gather | bytes 73728 | tf_op jit(solution)/shard_map/all_gather | solution.py:128
  93.4 0.7 copy.30
  94.1 0.3 fusion.53
  94.4 0.3 fusion.20
  94.7 9.3 %all_gather.18 = bf16[128,512]{1,0:T(8,128)(2,1)} all-gather(bf16[128,128]{1,0:T(8,128)(2,1)S(1)} %fusion.20), channel_id=1, replica_groups=mesh['ep'=8,'tp'=4] {'tp'}, dimensions={1}, use_global_device_ids=true | all-gather | bytes 163840 | tf_op jit(solution)/shard_map/all_gather | solution.py:176
  104.1 0.6 pad_clamp_fusion
  104.7 0.1 multiply_cosine_fusion.1
  104.8 0.4 fusion.34
  105.2 0.3 fusion.41
  105.5 0.0 all-gather.3.cloned.1.call-done
  105.6 1.7 %convolution_convert_fusion.1 = bf16[1024,256]{0,1:T(8,128)(2,1)S(1)} fusion(bf16[1024,512]{1,0:T(8,128)(2,1)} %all-gather.3.cloned.1.call-done, bf16[512,256]{1,0:T(8,128)(2,1)S(1)} %copy-done.7), kind=kOutput, calls=%fused_computation.18 | convolution fusion | flops 268697600 | bytes 1835008 | tf_op jit(solution)/shard_map/while/body/eval_jaxpr/dot_general | solution.py:116
  107.3 0.5 fusion.52
  107.8 2.0 %fusion.51 = (f32[4,128]{1,0:T(4,128)S(1)}, f32[4,128,1024]{2,1,0:T(8,128)S(1)}) fusion(f32[4,128,1024]{2,1,0:T(8,128)S(1)} %fusion.52, f32[128,4,16]{0,2,1:T(8,128)S(1)} %get-tuple-element.27, f32[128,4,16]{0,2,1:T(8,128)S(1)} %get-tuple-element.26, f32[1024,16]{0,1:T(8,128)S(1)} %get-tuple-element.25, f32[1024,16]{0,1:T(8,128)S(1)} %get-tuple-element.24), kind=kOutput, calls=%fused_computation.94 | convolution fusion | flops 202948096 | bytes 4392960 | tf_op jit(solution)/shard_map/while/body/eval_jaxpr/qhr,kr->hqk/dot_general | solution.py:100
  109.8 0.0 copy-start.8
  109.8 0.5 fusion.7
  110.3 0.7 copy-done.1
  111.0 0.0 copy-done.8
  111.1 1.3 convolution_convert_fusion
  112.3 9.5 %all-gather.5.cloned.1.call-done = bf16[384,4096]{1,0:T(8,128)(2,1)} async-done(((bf16[384,1024]{1,0:T(8,128)(2,1)}), bf16[384,4096]{1,0:T(8,128)(2,1)}) %all-gather.5.cloned.1.call-update) | async-done | bytes 3145744 | tf_op jit(solution)/shard_map/all_gather | solution.py:175
  121.8 5.7 %fusion.11 = bf16[384,512]{1,0:T(8,128)(2,1)} fusion(bf16[384,4096]{1,0:T(8,128)(2,1)} %all-gather.5.cloned.1.call-done, bf16[1,4096,512]{2,1,0:T(8,128)(2,1)} %param.36), kind=kOutput, calls=%fused_computation.19 | convolution fusion | flops 1610809344 | bytes 7733248 | tf_op jit(solution)/shard_map/dot_general | solution.py:178
  127.5 4.6 %all-to-all-start.1 = ((bf16[8,48,512]{2,1,0:T(8,128)(2,1)}), bf16[8,48,512]{2,1,0:T(8,128)(2,1)S(1)}, u32[]{:S(2)}, u32[]{:S(2)}) async-start(bf16[8,48,512]{2,1,0:T(8,128)(2,1)} %bitcast.78), calls=%async_computation.1 | async-start | bytes 786432 | tf_op jit(solution)/shard_map/all_to_all | solution.py:182
  132.1 1.6 %fusion.19 = bf16[128,4,64]{0,2,1:T(8,128)(2,1)S(1)} fusion(bf16[1024,4,64]{0,2,1:T(8,128)(2,1)} %bitcast.74, f32[4,128,1024]{2,1,0:T(8,128)S(1)} %get-tuple-element.44, f32[4,128]{1,0:T(4,128)S(1)} %get-tuple-element.29, f32[128,4]{0,1:T(4,128)S(1)} %bitcast_add_fusion.1, f32[128,4]{0,1:T(4,128)S(1)} %get-tuple-element.28), kind=kOutput, calls=%fused_computation.29 | convolution fusion | flops 68255744 | bytes 2693120 | tf_op jit(solution)/shard_map/while/body/eval_jaxpr/hqk,khe->hqe/dot_general | solution.py:106
  133.8 8.9 %all_gather.17 = bf16[128,1024]{0,1:T(8,128)(2,1)S(1)} all-gather(bf16[128,256]{0,1:T(8,128)(2,1)S(1)} %bitcast.79), channel_id=1, replica_groups=mesh['ep'=8,'tp'=4] {'tp'}, dimensions={1}, use_global_device_ids=true | all-gather | bytes 327680 | tf_op jit(solution)/shard_map/all_gather | solution.py:138
  142.7 1.0 convolution_convert_fusion.2
  143.7 1.0 all-to-all-done.1
  144.6 1.3 gather_fusion.1
  145.9 0.3 reshape.200
  146.3 0.7 multiply_reduce_fusion
  147.0 0.9 fusion.16
  (42 shorter events, 0.2 us)
Async XLA Ops:
  7.2 135.5 %copy-start = (bf16[1024,512]{1,0:T(8,128)(2,1)S(1)}, bf16[1024,512]{1,0:T(8,128)(2,1)}, u32[]{:S(2)}) copy-start(bf16[1024,512]{1,0:T(8,128)(2,1)} %param.29) | copy-start | bytes 3145732
  18.8 6.5 %copy-start.4 = (bf16[128,512]{1,0:T(8,128)(2,1)S(1)}, bf16[128,512]{1,0:T(8,128)(2,1)}, u32[]{:S(2)}) copy-start(bf16[128,512]{1,0:T(8,128)(2,1)} %param.21) | copy-start | bytes 393220
  18.8 6.7 %copy-start.11 = (f32[512]{0:T(512)S(1)}, f32[512]{0:T(512)}, u32[]{:S(2)}) copy-start(f32[512]{0:T(512)} %param.24) | copy-start | bytes 6148
  18.8 52.7 %all-to-all-start = ((bf16[8,48,2048]{2,1,0:T(8,128)(2,1)}), bf16[8,48,2048]{2,1,0:T(8,128)(2,1)S(1)}, u32[]{:S(2)}, u32[]{:S(2)}) async-start(bf16[8,48,2048]{2,1,0:T(8,128)(2,1)} %bitcast.14), calls=%async_computation | async-start | bytes 3145728 | tf_op jit(solution)/shard_map/all_to_all | solution.py:163
  25.3 80.2 %all-gather.3.cloned.1.call-start = ((), (), s32[]{:S(2)}) async-start(), calls=%async_computation.2 | async-start | bytes 1179648 | tf_op jit(solution)/shard_map/all_gather | solution.py:127
  26.3 95.6 %all-gather.5.cloned.1.call-start = ((), (), s32[]{:S(2)}) async-start(), calls=%async_computation.3 | async-start | bytes 3932160 | tf_op jit(solution)/shard_map/all_gather | solution.py:175
  71.5 4.2 %copy-start.13 = (bf16[1,2048,1024]{2,1,0:T(8,128)(2,1)S(1)}, bf16[1,2048,1024]{2,1,0:T(8,128)(2,1)}, u32[]{:S(2)}) copy-start(bf16[1,2048,1024]{2,1,0:T(8,128)(2,1)} %param.35) | copy-start | bytes 12582916
  75.7 2.9 %copy-start.6 = (bf16[128,1536]{1,0:T(8,128)(2,1)S(1)}, bf16[128,1536]{1,0:T(8,128)(2,1)}, u32[]{:S(2)}) copy-start(bf16[128,1536]{1,0:T(8,128)(2,1)} %param.20) | copy-start | bytes 1179652
  75.7 3.1 %copy-start.16 = (f32[1536]{0:T(1024)S(1)}, f32[1536]{0:T(1024)}, u32[]{:S(2)}) copy-start(f32[1536]{0:T(1024)} %param.23) | copy-start | bytes 18436
  78.6 1.9 %copy-start.10 = (bf16[128,32]{0,1:T(8,128)(2,1)S(1)}, bf16[128,32]{0,1:T(8,128)(2,1)}, u32[]{:S(2)}) copy-start(bf16[128,32]{0,1:T(8,128)(2,1)} %param.22) | copy-start | bytes 24580
  78.6 14.8 %copy-start.12 = (f32[128,2]{0,1:T(2,128)S(1)}, f32[128,2]{0,1:T(2,128)}, u32[]{:S(2)}) copy-start(f32[128,2]{0,1:T(2,128)} %param.33) | copy-start | bytes 3076
  78.6 15.5 %copy-start.2 = (bf16[2048,128]{1,0:T(8,128)(2,1)S(1)}, bf16[2048,128]{1,0:T(8,128)(2,1)}, u32[]{:S(2)}) copy-start(bf16[2048,128]{1,0:T(8,128)(2,1)} %param.37) | copy-start | bytes 1572868
  78.6 15.8 %copy-start.14 = (bf16[2048,128]{1,0:T(8,128)(2,1)S(1)}, bf16[2048,128]{1,0:T(8,128)(2,1)}, u32[]{:S(2)}) copy-start(bf16[2048,128]{1,0:T(8,128)(2,1)} %param.38) | copy-start | bytes 1572868
  80.5 25.0 %copy-start.7 = (bf16[512,256]{1,0:T(8,128)(2,1)S(1)}, bf16[512,256]{1,0:T(8,128)(2,1)}, u32[]{:S(2)}) copy-start(bf16[512,256]{1,0:T(8,128)(2,1)} %param.27) | copy-start | bytes 786436
  94.1 10.7 %copy-start.15 = (bf16[1536,128]{1,0:T(8,128)(2,1)S(1)}, bf16[1536,128]{1,0:T(8,128)(2,1)}, u32[]{:S(2)}) copy-start(bf16[1536,128]{1,0:T(8,128)(2,1)} %param.26) | copy-start | bytes 1179652
  109.8 1.2 copy-start.1
  109.8 1.3 copy-start.8
  127.5 17.1 %all-to-all-start.1 = ((bf16[8,48,512]{2,1,0:T(8,128)(2,1)}), bf16[8,48,512]{2,1,0:T(8,128)(2,1)S(1)}, u32[]{:S(2)}, u32[]{:S(2)}) async-start(bf16[8,48,512]{2,1,0:T(8,128)(2,1)} %bitcast.78), calls=%async_computation.1 | async-start | bytes 786432 | tf_op jit(solution)/shard_map/all_to_all | solution.py:182
  142.7 3.6 %copy-start.9 = (f32[128,2]{1,0:T(8,128)S(1)}, f32[128,2]{1,0:T(8,128)}, u32[]{:S(2)}) copy-start(f32[128,2]{1,0:T(8,128)} %copy.30) | copy-start | bytes 3076
  143.7 3.3 %copy-start.3 = (bf16[512,512]{1,0:T(8,128)(2,1)S(1)}, bf16[512,512]{1,0:T(8,128)(2,1)}, u32[]{:S(2)}) copy-start(bf16[512,512]{1,0:T(8,128)(2,1)} %param.39) | copy-start | bytes 1572868
  143.7 3.3 %copy-start.5 = (bf16[128,512]{1,0:T(8,128)(2,1)S(1)}, bf16[128,512]{1,0:T(8,128)(2,1)}, u32[]{:S(2)}) copy-start(bf16[128,512]{1,0:T(8,128)(2,1)} %all_gather.18) | copy-start | bytes 393220
Sparse Core Ops, SparseCore 0:
  28.3 37.9 all-gather.2
  78.7 43.0 all-gather.4
where the time goes:
time: 155 us
  waiting for transfers between devices  55.7 us (36%)
  blocking collectives  31.1 us (20%)
  matrix products  24.2 us (16%)
  between operations  14.4 us (9%)
  starting transfers between devices  11.2 us (7%)
  local copies, waits for them, and re-layouts  9.52 us (6%)
  other arithmetic  8.67 us (6%)
    all_to_all x1, waiting for transfers between devices, per_device(): lax.all_to_all(outgoing, 'ep', split_axis=0, concat_axis=0, tiled=True)  45.2 us
    all_gather x1, blocking collectives, per_device(): lax.all_gather(rotary_key, 'ep', axis=0, tiled=True)  12.8 us
    all_gather x1, waiting for transfers between devices, per_device(): lax.all_gather(hidden, 'tp', axis=1, tiled=True)  9.5 us
    all_gather x1, blocking collectives, per_device(): lax.all_gather(shared_hidden, 'tp', axis=1, tiled=True)  9.33 us
    all_gather x1, blocking collectives, per_device(): all_heads = lax.all_gather(heads_out, 'tp', axis=1, tiled=True)  8.93 us
    all_to_all x1, starting transfers between devices, per_device(): lax.all_to_all(outgoing, 'ep', split_axis=0, concat_axis=0, tiled=True)  6.49 us
    dot_general x1, matrix products, per_device(): jnp.dot(all_hidden, expert_down[0], preferred_element_type=jnp.float32)  5.67 us
    all_to_all x1, starting transfers between devices, per_device(): lax.all_to_all(expert_rows.reshape(experts, capacity, features), 'ep', sp...  4.62 us
  transfers between devices with their start and end apart: 4, of which 3 were waited for; matrix products, arithmetic and copies ran while one was open for 14% of the time, Pallas kernels for 0%

commit v1 on v0

--- a/solution.py
+++ b/solution.py
@@ -173,7 +173,7 @@
     ).astype(jnp.bfloat16)
     all_hidden, all_shared = (
         lax.all_gather(hidden, "tp", axis=1, tiled=True),
-        lax.all_gather(shared_hidden, "tp", axis=1, tiled=True),
+        jnp.concatenate(lax.all_gather(shared_hidden, axis_name="tp"), axis=1),
     )
     expert_rows = jnp.dot(all_hidden, expert_down[0], preferred_element_type=jnp.float32).astype(
         jnp.bfloat16

time: 155 us -> 155 us (level)
  transfers between devices with their start and end apart: 4 -> 4, of which waited for: 3 -> 3; matrix products, arithmetic and copies ran while one was open for 14% -> 15% of each run, Pallas kernels for 0% -> 0%
where the time goes in v1:
time: 155 us
  waiting for transfers between devices  54.8 us (35%)
  blocking collectives  30.3 us (20%)
  matrix products  25.2 us (16%)
  between operations  14.4 us (9%)
  starting transfers between devices  11.2 us (7%)
  local copies, waits for them, and re-layouts  10.3 us (7%)
  other arithmetic  8.67 us (6%)
    all_to_all x1, waiting for transfers between devices, per_device(): lax.all_to_all(outgoing, 'ep', split_axis=0, concat_axis=0, tiled=True)  45.2 us
    all_gather x1, blocking collectives, per_device(): lax.all_gather(rotary_key, 'ep', axis=0, tiled=True)  12.7 us
    all_gather x1, blocking collectives, per_device(): all_heads = lax.all_gather(heads_out, 'tp', axis=1, tiled=True)  8.94 us
    all_gather x1, waiting for transfers between devices, per_device(): lax.all_gather(hidden, 'tp', axis=1, tiled=True)  8.65 us
    all_gather x1, blocking collectives, per_device(): lax.all_gather(shared_hidden, axis_name='tp')  8.64 us
    all_to_all x1, starting transfers between devices, per_device(): lax.all_to_all(outgoing, 'ep', split_axis=0, concat_axis=0, tiled=True)  6.49 us
    dot_general x1, matrix products, per_device(): jnp.dot(all_hidden, expert_down[0], preferred_element_type=jnp.float32)  5.67 us
    all_to_all x1, starting transfers between devices, per_device(): lax.all_to_all(expert_rows.reshape(experts, capacity, features), 'ep', sp...  4.6 us
  transfers between devices with their start and end apart: 4, of which 3 were waited for; matrix products, arithmetic and copies ran while one was open for 15% of the time, Pallas kernels for 0%

profile of v1, /device:TPU:0, one launch (start us, length us, event | category | flops | bytes accessed | tf_op | source)
XLA Modules:
  0.0 154.8 jit_solution(18038828729426986537)
XLA Ops:
  7.2 0.0 copy-start
  7.2 0.9 copy.29
  8.1 0.1 eq.29
  8.2 0.1 eq.25
  8.3 0.7 broadcast_multiply_fusion
  9.0 0.6 reduce-window.6
  9.6 0.2 slice_reduce_fusion
  9.9 0.1 copy.28
  10.0 0.1 mul.279
  10.1 0.1 fusion.46
  10.2 1.4 scatter_custom_fusion
  11.7 1.2 convert_reduce_fusion
  12.9 1.3 fusion.21
  14.2 1.4 fusion.23
  15.6 0.1 concatenate.12
  15.7 3.1 %gather_fusion = bf16[384,2048]{1,0:T(8,128)(2,1)} fusion(bf16[129,2048]{1,0:T(8,128)(2,1)S(1)} %concatenate.12, s32[1024]{0:T(1024)S(1)} %pad_clamp_fusion.1), kind=kCustom, calls=%fused_computation | custom fusion | bytes 3147264 | tf_op jit(solution)/shard_map/gather | solution.py:162
  18.8 6.5 %all-to-all-start = ((bf16[8,48,2048]{2,1,0:T(8,128)(2,1)}), bf16[8,48,2048]{2,1,0:T(8,128)(2,1)S(1)}, u32[]{:S(2)}, u32[]{:S(2)}) async-start(bf16[8,48,2048]{2,1,0:T(8,128)(2,1)} %bitcast.17), calls=%async_computation | async-start | bytes 3145728 | tf_op jit(solution)/shard_map/all_to_all | solution.py:163
  25.3 0.0 all-gather.4.cloned.1.call-start
  25.4 0.1 fusion.29
  25.5 0.0 copy-done.11
  25.5 0.8 fusion.31
  26.2 0.0 all-gather.4.cloned.1.call-update
  26.3 0.0 all-gather.6.cloned.1.call-start
  26.3 45.2 %all-to-all-done = bf16[8,48,2048]{2,1,0:T(8,128)(2,1)S(1)} async-done(((bf16[8,48,2048]{2,1,0:T(8,128)(2,1)}), bf16[8,48,2048]{2,1,0:T(8,128)(2,1)S(1)}, u32[]{:S(2)}, u32[]{:S(2)}) %all-to-all-start) | async-done | bytes 1572896 | tf_op jit(solution)/shard_map/all_to_all | solution.py:163
  71.5 4.1 %fusion.4 = f32[384,1024]{1,0:T(8,128)S(1)} fusion(bf16[384,2048]{1,0:T(8,128)(2,1)S(1)} %bitcast.80, bf16[1,2048,1024]{2,1,0:T(8,128)(2,1)} %param.34), kind=kOutput, calls=%fused_computation.7 | convolution fusion | flops 1610612736 | bytes 7340032 | tf_op jit(solution)/shard_map/dot_general | solution.py:167
  75.7 0.0 copy-start.6
  75.7 0.0 copy-start.15
  75.7 2.9 %multiply_convert_fusion = bf16[384,1024]{1,0:T(8,128)(2,1)} fusion(f32[384,1024]{1,0:T(8,128)S(1)} %fusion.4, bf16[384,2048]{1,0:T(8,128)(2,1)S(1)} %bitcast.81, bf16[1,2048,1024]{2,1,0:T(8,128)(2,1)S(1)} %copy-done.13), kind=kOutput, calls=%fused_computation.14 | convolution fusion | flops 1612972032 | bytes 8126464 | tf_op jit(solution)/shard_map/dot_general | solution.py:168
  78.6 0.0 all-gather.6.cloned.1.call-update
  78.6 0.0 copy-done.6
  78.6 0.2 fusion.26
  78.8 1.6 %convolution_convert_fusion.3 = bf16[128,256]{1,0:T(8,128)(2,1)S(1)} fusion(bf16[1536,256]{1,0:T(8,128)(2,1)} %param.25, bf16[128,1536]{1,0:T(8,128)(2,1)S(1)} %copy-done.6, f32[1536]{0:T(1024)S(1)} %copy-done.15, f32[128]{0:T(128)S(1)} %add_rsqrt_fusion.2), kind=kOutput, calls=%fused_computation.28 | convolution fusion | flops 101482496 | bytes 1251840 | tf_op jit(solution)/shard_map/dot_general | solution.py:77
  80.4 0.1 copy.25
  80.5 12.7 %all_gather.19 = bf16[1024,32]{0,1:T(8,128)(2,1)S(1)} all-gather(bf16[128,32]{0,1:T(8,128)(2,1)S(1)} %copy-done.10), channel_id=1, replica_groups=mesh['ep'=8,'tp'=4] {'ep'}, dimensions={0}, use_global_device_ids=true | all-gather | bytes 73728 | tf_op jit(solution)/shard_map/all_gather | solution.py:128
  93.3 0.0 copy-start.7
  93.3 0.7 copy.31
  94.0 0.3 fusion.53
  94.3 0.3 fusion.20
  94.6 8.6 %all-gather = bf16[512,128]{1,0:T(8,128)(2,1)S(1)} all-gather(bf16[128,128]{1,0:T(8,128)(2,1)S(1)} %fusion.20), channel_id=2, replica_groups=mesh['ep'=8,'tp'=4] {'tp'}, dimensions={0}, use_global_device_ids=true | all-gather | bytes 163840 | tf_op jit(solution)/shard_map/all_gather | solution.py:176
  103.2 0.8 copy.27
  104.0 0.6 pad_clamp_fusion
  104.6 0.1 multiply_cosine_fusion.1
  104.7 1.4 fusion.34
  106.1 0.3 fusion.41
  106.5 0.0 all-gather.4.cloned.1.call-done
  106.5 1.7 %convolution_convert_fusion.1 = bf16[1024,256]{0,1:T(8,128)(2,1)S(1)} fusion(bf16[1024,512]{1,0:T(8,128)(2,1)} %all-gather.4.cloned.1.call-done, bf16[512,256]{1,0:T(8,128)(2,1)S(1)} %copy-done.7), kind=kOutput, calls=%fused_computation.18 | convolution fusion | flops 268697600 | bytes 1835008 | tf_op jit(solution)/shard_map/while/body/eval_jaxpr/dot_general | solution.py:116
  108.2 0.5 fusion.52
  108.7 2.0 %fusion.51 = (f32[4,128]{1,0:T(4,128)S(1)}, f32[4,128,1024]{2,1,0:T(8,128)S(1)}) fusion(f32[4,128,1024]{2,1,0:T(8,128)S(1)} %fusion.52, f32[128,4,16]{0,2,1:T(8,128)S(1)} %get-tuple-element.27, f32[128,4,16]{0,2,1:T(8,128)S(1)} %get-tuple-element.26, f32[1024,16]{0,1:T(8,128)S(1)} %get-tuple-element.25, f32[1024,16]{0,1:T(8,128)S(1)} %get-tuple-element.24), kind=kOutput, calls=%fused_computation.94 | convolution fusion | flops 202948096 | bytes 4392960 | tf_op jit(solution)/shard_map/while/body/eval_jaxpr/qhr,kr->hqk/dot_general | solution.py:100
  110.7 0.0 copy-start.8
  110.8 0.5 fusion.7
  111.2 0.7 copy-done.1
  112.0 0.0 copy-done.8
  112.0 1.3 convolution_convert_fusion
  113.3 8.6 %all-gather.6.cloned.1.call-done = bf16[384,4096]{1,0:T(8,128)(2,1)} async-done(((bf16[384,1024]{1,0:T(8,128)(2,1)}), bf16[384,4096]{1,0:T(8,128)(2,1)}) %all-gather.6.cloned.1.call-update) | async-done | bytes 3145744 | tf_op jit(solution)/shard_map/all_gather | solution.py:175
  121.9 5.7 %fusion.11 = bf16[384,512]{1,0:T(8,128)(2,1)} fusion(bf16[384,4096]{1,0:T(8,128)(2,1)} %all-gather.6.cloned.1.call-done, bf16[1,4096,512]{2,1,0:T(8,128)(2,1)} %param.36), kind=kOutput, calls=%fused_computation.19 | convolution fusion | flops 1610809344 | bytes 7733248 | tf_op jit(solution)/shard_map/dot_general | solution.py:178
  127.6 4.6 %all-to-all-start.1 = ((bf16[8,48,512]{2,1,0:T(8,128)(2,1)}), bf16[8,48,512]{2,1,0:T(8,128)(2,1)S(1)}, u32[]{:S(2)}, u32[]{:S(2)}) async-start(bf16[8,48,512]{2,1,0:T(8,128)(2,1)} %bitcast.84), calls=%async_computation.1 | async-start | bytes 786432 | tf_op jit(solution)/shard_map/all_to_all | solution.py:182
  132.2 1.6 %fusion.19 = bf16[128,4,64]{0,2,1:T(8,128)(2,1)S(1)} fusion(bf16[1024,4,64]{0,2,1:T(8,128)(2,1)} %bitcast.78, f32[4,128,1024]{2,1,0:T(8,128)S(1)} %get-tuple-element.44, f32[4,128]{1,0:T(4,128)S(1)} %get-tuple-element.29, f32[128,4]{0,1:T(4,128)S(1)} %bitcast_add_fusion.1, f32[128,4]{0,1:T(4,128)S(1)} %get-tuple-element.28), kind=kOutput, calls=%fused_computation.29 | convolution fusion | flops 68255744 | bytes 2693120 | tf_op jit(solution)/shard_map/while/body/eval_jaxpr/hqk,khe->hqe/dot_general | solution.py:106
  133.8 8.9 %all_gather.20 = bf16[128,1024]{0,1:T(8,128)(2,1)S(1)} all-gather(bf16[128,256]{0,1:T(8,128)(2,1)S(1)} %bitcast.85), channel_id=1, replica_groups=mesh['ep'=8,'tp'=4] {'tp'}, dimensions={1}, use_global_device_ids=true | all-gather | bytes 327680 | tf_op jit(solution)/shard_map/all_gather | solution.py:138
  142.8 1.0 convolution_convert_fusion.2
  143.8 0.9 all-to-all-done.1
  144.7 1.3 gather_fusion.1
  146.0 0.3 reshape.208
  146.4 0.7 multiply_reduce_fusion
  147.1 0.9 fusion.16
  (41 shorter events, 0.2 us)
Async XLA Ops:
  7.2 135.6 %copy-start = (bf16[1024,512]{1,0:T(8,128)(2,1)S(1)}, bf16[1024,512]{1,0:T(8,128)(2,1)}, u32[]{:S(2)}) copy-start(bf16[1024,512]{1,0:T(8,128)(2,1)} %param.29) | copy-start | bytes 3145732
  18.8 6.5 %copy-start.4 = (bf16[128,512]{1,0:T(8,128)(2,1)S(1)}, bf16[128,512]{1,0:T(8,128)(2,1)}, u32[]{:S(2)}) copy-start(bf16[128,512]{1,0:T(8,128)(2,1)} %param.21) | copy-start | bytes 393220
  18.8 6.7 %copy-start.11 = (f32[512]{0:T(512)S(1)}, f32[512]{0:T(512)}, u32[]{:S(2)}) copy-start(f32[512]{0:T(512)} %param.24) | copy-start | bytes 6148
  18.8 52.7 %all-to-all-start = ((bf16[8,48,2048]{2,1,0:T(8,128)(2,1)}), bf16[8,48,2048]{2,1,0:T(8,128)(2,1)S(1)}, u32[]{:S(2)}, u32[]{:S(2)}) async-start(bf16[8,48,2048]{2,1,0:T(8,128)(2,1)} %bitcast.17), calls=%async_computation | async-start | bytes 3145728 | tf_op jit(solution)/shard_map/all_to_all | solution.py:163
  25.3 81.2 %all-gather.4.cloned.1.call-start = ((), (), s32[]{:S(2)}) async-start(), calls=%async_computation.2 | async-start | bytes 1179648 | tf_op jit(solution)/shard_map/all_gather | solution.py:127
  26.3 95.6 %all-gather.6.cloned.1.call-start = ((), (), s32[]{:S(2)}) async-start(), calls=%async_computation.3 | async-start | bytes 3932160 | tf_op jit(solution)/shard_map/all_gather | solution.py:175
  71.5 4.2 %copy-start.13 = (bf16[1,2048,1024]{2,1,0:T(8,128)(2,1)S(1)}, bf16[1,2048,1024]{2,1,0:T(8,128)(2,1)}, u32[]{:S(2)}) copy-start(bf16[1,2048,1024]{2,1,0:T(8,128)(2,1)} %param.35) | copy-start | bytes 12582916
  75.7 2.9 %copy-start.6 = (bf16[128,1536]{1,0:T(8,128)(2,1)S(1)}, bf16[128,1536]{1,0:T(8,128)(2,1)}, u32[]{:S(2)}) copy-start(bf16[128,1536]{1,0:T(8,128)(2,1)} %param.20) | copy-start | bytes 1179652
  75.7 3.1 %copy-start.15 = (f32[1536]{0:T(1024)S(1)}, f32[1536]{0:T(1024)}, u32[]{:S(2)}) copy-start(f32[1536]{0:T(1024)} %param.23) | copy-start | bytes 18436
  78.6 1.9 %copy-start.10 = (bf16[128,32]{0,1:T(8,128)(2,1)S(1)}, bf16[128,32]{0,1:T(8,128)(2,1)}, u32[]{:S(2)}) copy-start(bf16[128,32]{0,1:T(8,128)(2,1)} %param.22) | copy-start | bytes 24580
  78.6 14.7 %copy-start.12 = (f32[128,2]{0,1:T(2,128)S(1)}, f32[128,2]{0,1:T(2,128)}, u32[]{:S(2)}) copy-start(f32[128,2]{0,1:T(2,128)} %param.33) | copy-start | bytes 3076
  78.6 15.4 %copy-start.2 = (bf16[2048,128]{1,0:T(8,128)(2,1)S(1)}, bf16[2048,128]{1,0:T(8,128)(2,1)}, u32[]{:S(2)}) copy-start(bf16[2048,128]{1,0:T(8,128)(2,1)} %param.37) | copy-start | bytes 1572868
  78.6 15.7 %copy-start.14 = (bf16[2048,128]{1,0:T(8,128)(2,1)S(1)}, bf16[2048,128]{1,0:T(8,128)(2,1)}, u32[]{:S(2)}) copy-start(bf16[2048,128]{1,0:T(8,128)(2,1)} %param.38) | copy-start | bytes 1572868
  93.3 13.2 %copy-start.7 = (bf16[512,256]{1,0:T(8,128)(2,1)S(1)}, bf16[512,256]{1,0:T(8,128)(2,1)}, u32[]{:S(2)}) copy-start(bf16[512,256]{1,0:T(8,128)(2,1)} %param.27) | copy-start | bytes 786436
  110.7 1.2 copy-start.1
  110.7 1.3 copy-start.8
  127.6 17.1 %all-to-all-start.1 = ((bf16[8,48,512]{2,1,0:T(8,128)(2,1)}), bf16[8,48,512]{2,1,0:T(8,128)(2,1)S(1)}, u32[]{:S(2)}, u32[]{:S(2)}) async-start(bf16[8,48,512]{2,1,0:T(8,128)(2,1)} %bitcast.84), calls=%async_computation.1 | async-start | bytes 786432 | tf_op jit(solution)/shard_map/all_to_all | solution.py:182
  142.8 3.6 %copy-start.9 = (f32[128,2]{1,0:T(8,128)S(1)}, f32[128,2]{1,0:T(8,128)}, u32[]{:S(2)}) copy-start(f32[128,2]{1,0:T(8,128)} %copy.31) | copy-start | bytes 3076
  143.8 3.3 %copy-start.3 = (bf16[512,512]{1,0:T(8,128)(2,1)S(1)}, bf16[512,512]{1,0:T(8,128)(2,1)}, u32[]{:S(2)}) copy-start(bf16[512,512]{1,0:T(8,128)(2,1)} %param.39) | copy-start | bytes 1572868
  143.8 3.3 %copy-start.5 = (bf16[4,128,128]{1,2,0:T(8,128)(2,1)S(1)}, bf16[4,128,128]{1,2,0:T(8,128)(2,1)}, u32[]{:S(2)}) copy-start(bf16[4,128,128]{1,2,0:T(8,128)(2,1)} %copy.27) | copy-start | bytes 393220
Sparse Core Ops, SparseCore 0:
  28.3 37.9 all-gather.3
  78.7 43.1 all-gather.5
